TPU v7x, 256 devices: a whole 4x4x8 slice. The times are simulated.
256 devices in a mesh: sp: 16 (over y, x), tp: 16 (over z, core).
Axes of the slice: x: 4, y: 4, z: 8, core: 2. Of those that a mesh axis runs over, the one named last changes fastest.
Arguments:
- residual: bfloat16 [8192, 2048], P(('sp', 'tp')), may hold values from -6 to 6
- queries: bfloat16 [8192, 4096], P('sp', 'tp'), may hold values from -6 to 6
- keys: bfloat16 [8192, 4096], P('sp', 'tp'), may hold values from -6 to 6
- values: bfloat16 [8192, 4096], P('sp', 'tp'), may hold values from -6 to 6
- in_gate: float32 [16, 8192], P('tp', 'sp'), may hold values from -5 to 130
- forget_gate: float32 [16, 8192], P('tp', 'sp'), may hold values from 0 to 16
- doc_ids: int32 [8192], P('sp'), may hold values from 0 to 7, never falling along the last dimension, each value on 1 to 4096 neighbouring positions
- head_gain: float32 [4096], P('tp'), may hold values from 0.1 to 1.9
- out_weight: bfloat16 [4096, 2048], P('tp'), may hold values from -0.09375 to 0.09375
- norm_gain: float32 [2048], replicated, may hold values from 0.1 to 1.9
- route_ids: int32 [8192, 2], P(('sp', 'tp')), may hold values from 0 to 15, all different within a row; in each aligned block of 32 rows (0 to 31, 32 to 63, ...) at most 5 rows name the same one
- route_weights: float32 [8192, 2], P(('sp', 'tp')), may hold values from 0.2 to 1
- gate_proj: bfloat16 [16, 2048, 4096], P('sp', None, 'tp'), may hold values from -0.125 to 0.125
- up_proj: bfloat16 [16, 2048, 4096], P('sp', None, 'tp'), may hold values from -0.125 to 0.125
- down_proj: bfloat16 [16, 4096, 2048], P('sp', 'tp'), may hold values from -0.09375 to 0.09375
Outputs:
- mixed: bfloat16 [8192, 2048], P(('sp', 'tp'))
Inputs may be any that keep to these rules, and one draw needn't show every extreme that they name: `route_ids`: each row names 2 different experts. In each aligned block of 32 rows (the rows of one device) no expert is named by more than 5 rows, and in some blocks one expert by exactly 5. `doc_ids`: numbers never fall along the sequence; no document covers more than half of the 8192 positions, and one covers exactly half.
All inputs are finite; a program needn't handle non-finite values.
Results may differ from a plain program's by a relative error of at most 0.018.
Values may be sent and summed in bfloat16 or wider, within the bound.
A program may use at most 64 MiB of HBM per device.

v0:
```python
import math

import jax
import jax.numpy as jnp
from jax import lax
from jax.sharding import Mesh
from jax.sharding import PartitionSpec as P

SP = ("sp_0", "sp_1")
SP_TP = ("sp_0", "sp_1", "tp")


MASKED = -1e30
EPSILON = 1e-06


def neutral_like(value, identity):
    return jax.tree.map(
        lambda a, e: jnp.broadcast_to(jnp.asarray(e, a.dtype), a.shape), value, identity
    )


def carried_in(value, axes, combine, identity):
    before = start = neutral_like(value, identity)
    running = value
    for axis in reversed(axes):
        peers, index = (lax.axis_size(axis), lax.axis_index(axis))
        pieces = jax.tree.map(lambda part: lax.all_gather(part, axis), running)
        inside, running = (start, start)
        for k in range(peers):
            passed = k < index
            running = combine(running, jax.tree.map(lambda part: part[k], pieces))
            inside = jax.tree.map(lambda new, old: jnp.where(passed, new, old), running, inside)
        before = combine(inside, before)
    return before


def block_step(state, pieces):
    memory, normalizer, max_level, carry_doc = state
    q_block, k_block, v_block, in_block, forget_block, doc_block = pieces
    scaling = q_block.shape[1] ** (-0.5)
    cum_forget = jnp.cumsum(forget_block)
    positions = jnp.arange(q_block.shape[0])
    permitted_mask = (positions[:, None] >= positions[None, :]) & (
        doc_block[:, None] == doc_block[None, :]
    )
    log_weights = jnp.where(
        permitted_mask, cum_forget[:, None] - cum_forget[None, :] + in_block[None, :], MASKED
    )
    carried = jnp.where(doc_block == carry_doc, cum_forget + max_level, MASKED)
    row_max = jnp.maximum(carried, jnp.max(log_weights, axis=1))
    scores = jnp.dot(q_block, k_block.T, preferred_element_type=jnp.float32) * scaling
    weighted = scores * jnp.exp(log_weights - row_max[:, None])
    carry_weight = jnp.exp(carried - row_max)
    query_scaled = q_block.astype(jnp.float32) * scaling
    key_full = k_block.astype(jnp.float32)
    value_full = v_block.astype(jnp.float32)
    readout_numerator = jnp.dot(weighted, value_full, precision=lax.Precision.HIGHEST)
    readout_numerator = readout_numerator + carry_weight[:, None] * jnp.dot(
        query_scaled, memory.T, precision=lax.Precision.HIGHEST
    )
    denominator = jnp.sum(weighted, axis=1) + carry_weight * jnp.dot(
        query_scaled, normalizer, precision=lax.Precision.HIGHEST
    )
    last_doc = doc_block[-1]
    forget_total = cum_forget[-1]
    log_end = jnp.where(doc_block == last_doc, forget_total - cum_forget + in_block, MASKED)
    carry_log = jnp.where(carry_doc == last_doc, forget_total + max_level, MASKED)
    new_max = jnp.maximum(carry_log, jnp.max(log_end))
    end_weight = jnp.exp(log_end - new_max)
    kept_share = jnp.exp(carry_log - new_max)
    new_memory = kept_share * memory + jnp.dot(
        (value_full * end_weight[:, None]).T, key_full, precision=lax.Precision.HIGHEST
    )
    new_normalizer = kept_share * normalizer + jnp.dot(
        end_weight, key_full, precision=lax.Precision.HIGHEST
    )
    return (
        (new_memory, new_normalizer, new_max, last_doc),
        (readout_numerator, denominator, row_max),
    )


def run_blocks(
    queries_in,
    keys_in,
    incoming_vectors,
    in_gates,
    log_forget,
    doc_row,
    memory,
    normalizer,
    max_level,
    carry_doc,
):
    extent = queries_in.shape[0]
    block_size = math.gcd(extent, 256)
    blocks = extent // block_size

    def to_blocks(tensor):
        return tensor.reshape((blocks, block_size) + tensor.shape[1:])

    pieces = tuple(
        (
            to_blocks(tensor)
            for tensor in (queries_in, keys_in, incoming_vectors, in_gates, log_forget, doc_row)
        )
    )
    final_state, outputs = lax.scan(block_step, (memory, normalizer, max_level, carry_doc), pieces)
    readout_numerator, denominator, row_max = outputs
    return (
        readout_numerator.reshape(extent, -1),
        denominator.reshape(extent),
        row_max.reshape(extent),
        final_state,
    )


def combine_states(earlier, later):
    memory_a, normal_a, level_a, forget_a, first_a, last_a = earlier
    memory_b, normal_b, level_b, forget_b, first_b, last_b = later
    joined = (last_a == first_b) | (last_a < 0) | (first_b < 0)
    passed = forget_b + jnp.where(joined, 0.0, MASKED)
    new_level = jnp.maximum(passed + level_a, level_b)
    share_a = jnp.exp(passed + level_a - new_level)
    fraction_second = jnp.exp(level_b - new_level)
    new_memory = share_a[:, None, None] * memory_a + fraction_second[:, None, None] * memory_b
    new_normal = share_a[:, None] * normal_a + fraction_second[:, None] * normal_b
    first_doc = jnp.where(first_a < 0, first_b, first_a)
    last_doc = jnp.where(last_b < 0, last_a, last_b)
    return (new_memory, new_normal, new_level, forget_a + passed, first_doc, last_doc)


def on_device(
    residual,
    queries,
    keys,
    values,
    in_gate,
    forget_gate,
    doc_ids,
    head_gain,
    out_weight,
    norm_gain,
    route_ids,
    route_weights,
    gate_proj,
    up_proj,
    down_proj,
):
    extent, local_width = queries.shape
    heads_here = in_gate.shape[0]
    head_size = local_width // heads_here

    def by_head(tensor):
        return tensor.reshape(extent, heads_here, head_size).transpose(1, 0, 2)

    query_heads = by_head(queries)
    key_heads = by_head(keys)
    value_heads = by_head(values)
    log_forget = jax.nn.log_sigmoid(forget_gate)
    cum_forget = jnp.cumsum(log_forget, axis=1)
    first_doc = doc_ids[0]
    last_doc = doc_ids[-1]
    run_heads = jax.vmap(run_blocks, in_axes=(0, 0, 0, 0, 0, None, 0, 0, 0, None))
    forget_total = jnp.where(first_doc == last_doc, cum_forget[:, -1], MASKED)
    doc_first = first_doc.astype(jnp.float32).reshape(1)
    doc_last = last_doc.astype(jnp.float32).reshape(1)
    empty_memory = jnp.zeros((heads_here, head_size, head_size), jnp.float32)
    empty_normal = jnp.zeros((heads_here, head_size), jnp.float32)
    empty_level = jnp.full((heads_here,), MASKED, jnp.float32)
    identity = (
        empty_memory,
        empty_normal,
        empty_level,
        jnp.zeros((heads_here,), jnp.float32),
        jnp.full((1,), -1.0, jnp.float32),
        jnp.full((1,), -1.0, jnp.float32),
    )
    readout_numerator, denominator, row_max, final_state = run_heads(
        query_heads,
        key_heads,
        value_heads,
        in_gate,
        log_forget,
        doc_ids,
        empty_memory,
        empty_normal,
        empty_level,
        first_doc,
    )
    local_state = (
        final_state[0],
        final_state[1],
        final_state[2],
        forget_total,
        doc_first,
        doc_last,
    )
    incoming = carried_in(local_state, SP, combine_states, identity)
    linked = incoming[5][0] == doc_first[0]
    in_level = jnp.where(linked, incoming[2], MASKED)
    carried = jnp.where(doc_ids[None, :] == first_doc, cum_forget + in_level[:, None], MASKED)
    new_max = jnp.maximum(row_max, carried)
    own_share = jnp.exp(row_max - new_max)
    far_share = jnp.exp(carried - new_max)
    query_scaled = query_heads.astype(jnp.float32) * head_size ** (-0.5)
    readout_numerator = own_share[..., None] * readout_numerator + far_share[
        ..., None
    ] * jnp.einsum("htd,hvd->htv", query_scaled, incoming[0], precision=lax.Precision.HIGHEST)
    denominator = own_share * denominator + far_share * jnp.einsum(
        "htd,hd->ht", query_scaled, incoming[1], precision=lax.Precision.HIGHEST
    )
    mixed_heads = (
        readout_numerator / jnp.maximum(jnp.abs(denominator), jnp.exp(-new_max))[..., None]
    )
    normed_heads = mixed_heads * lax.rsqrt(
        jnp.mean(mixed_heads * mixed_heads, axis=-1, keepdims=True) + EPSILON
    )
    normed_heads = normed_heads * head_gain.reshape(heads_here, 1, head_size)
    head_rows = normed_heads.transpose(1, 0, 2).reshape(extent, local_width).astype(jnp.bfloat16)
    rows_here, model_width = residual.shape
    update = lax.psum_scatter(
        jnp.dot(head_rows, out_weight, preferred_element_type=jnp.float32).astype(jnp.bfloat16),
        "tp",
        scatter_dimension=0,
        tiled=True,
    ).astype(jnp.float32)
    stream = residual.astype(jnp.float32) + update
    normed = (
        stream * lax.rsqrt(jnp.mean(stream * stream, axis=-1, keepdims=True) + EPSILON) * norm_gain
    )
    normed = normed.astype(jnp.bfloat16)
    experts_all = gate_proj.shape[0] * lax.axis_size(SP)
    top_count = route_ids.shape[1]
    capacity = max(2, rows_here * top_count * 5 // (4 * experts_all))
    flat_ids = route_ids.reshape(-1)
    onehot = (flat_ids[:, None] == jnp.arange(experts_all, dtype=jnp.int32)[None, :]).astype(
        jnp.int32
    )
    earlier = jnp.cumsum(onehot, axis=0) - onehot
    slot_rank = jnp.sum(earlier * onehot, axis=1)
    slot_index = flat_ids * capacity + slot_rank
    placing = (
        slot_index[None, :] == jnp.arange(experts_all * capacity, dtype=jnp.int32)[:, None]
    ).astype(jnp.bfloat16)
    copies = jnp.repeat(normed, top_count, axis=0)
    outgoing = jnp.dot(placing, copies, preferred_element_type=jnp.float32).astype(jnp.bfloat16)
    outgoing = outgoing.reshape(experts_all, capacity, model_width)
    arrived = lax.all_to_all(outgoing, SP, split_axis=0, concat_axis=0, tiled=True).reshape(
        -1, model_width
    )
    piece = lax.all_gather(arrived, "tp", axis=0, tiled=True)
    gate_part = jnp.dot(piece, gate_proj[0], preferred_element_type=jnp.float32)
    up_part = jnp.dot(piece, up_proj[0], preferred_element_type=jnp.float32)
    hidden = (jax.nn.silu(gate_part) * up_part).astype(jnp.bfloat16)
    expert_sum = lax.psum_scatter(
        jnp.dot(hidden, down_proj[0], preferred_element_type=jnp.float32).astype(jnp.bfloat16),
        "tp",
        scatter_dimension=0,
        tiled=True,
    )
    expert_out = expert_sum.reshape(experts_all, capacity, model_width)
    returned = lax.all_to_all(expert_out, SP, split_axis=0, concat_axis=0, tiled=True)
    picked = jnp.take(returned.reshape(-1, model_width), slot_index, axis=0)
    picked = picked.reshape(rows_here, top_count, model_width)
    expert_mix = jnp.sum(route_weights[..., None] * picked.astype(jnp.float32), axis=1)
    return (stream + expert_mix).astype(jnp.bfloat16)


def solution(mesh):
    finer = Mesh(mesh.devices.reshape(4, 4, mesh.shape["tp"]), ("sp_0", "sp_1", "tp"))
    in_specs = (
        P(SP_TP, None),
        P(SP, "tp"),
        P(SP, "tp"),
        P(SP, "tp"),
        P("tp", SP),
        P("tp", SP),
        P(SP),
        P("tp"),
        P("tp", None),
        P(),
        P(SP_TP, None),
        P(SP_TP, None),
        P(SP, None, "tp"),
        P(SP, None, "tp"),
        P(SP, "tp", None),
    )
    out_specs = P(SP_TP, None)
    return jax.shard_map(
        on_device, mesh=finer, in_specs=in_specs, out_specs=out_specs, check_vma=False
    )
```

profile of v0, /device:TPU:2, one launch (start us, length us, event | category | flops | bytes accessed | tf_op | source)
XLA Modules:
  0.0 372.2 jit_solution(4518122679349654062)
XLA Ops:
  6.5 1.4 fusion.182
  10.0 25.1 %while.23 = (s32[]{:T(128)}, f32[1,256,256]{2,1,0:T(8,128)S(1)}, f32[1,256]{1,0:T(1,128)S(1)}, f32[1]{0:T(128)}, s32[]{:T(128)}, /*index=5*/f32[2,1,256,256]{3,2...) while((s32[]{:T(128)}, f32[1,256,256]{2,1,0:T(8,128)S(1)}, ...), condition=%wide.region_6.7_spmd.clone, body=%wide.region_0.6_spmd.clone.sunk | while | flops 641046528 | bytes 6349332 | solution.py:109
  13.2 1.3 fusion.226
  15.7 1.9 fusion.223
  17.6 1.3 fusion.227
  24.5 1.2 fusion.225
  25.7 1.3 fusion.226
  28.2 1.9 fusion.223
  30.1 1.3 fusion.227
  45.2 10.0 %all-reduce.8 = (f32[4]{0:T(128)S(1)}, f32[4]{0:T(128)S(1)}, f32[4]{0:T(128)S(1)}, f32[4]{0:T(128)S(1)}) all-reduce(f32[4]{0:T(128)S(1)} %dynamic-update-slice, f32[4]{0:T(128)S(1)} %fusion.156, f32[4]{0:T(128)S(1)} %dynamic-update-slice.3, f32[4]{0:T(128)S(1)} %dynamic-update-slice.6), channel_id=1, replica_groups=mesh['sp_0'=4,'sp_1'=4,'tp'=16] {'sp_1'}, use_global_device_ids=true, to_apply=%add | all-reduce | flops 16 | bytes 128
  55.9 2.6 fusion.152
  65.8 1.2 fusion.189
  72.3 2.0 fusion.70
  75.1 1.9 fusion.188
  78.2 1.4 dynamic-update-slice.7
  80.3 1.4 dynamic-update-slice.5
  81.8 1.4 dynamic-update-slice.1
  83.2 9.3 %all-reduce.9 = (f32[4]{0:T(128)S(1)}, f32[4]{0:T(128)S(1)}, f32[4]{0:T(128)S(1)}, f32[4]{0:T(128)S(1)}) all-reduce(f32[4]{0:T(128)S(1)} %dynamic-update-slice.1, f32[4]{0:T(128)S(1)} %dynamic-update-slice.4, f32[4]{0:T(128)S(1)} %dynamic-update-slice.5, f32[4]{0:T(128)S(1)} %dynamic-update-slice.7), channel_id=2, replica_groups=mesh['sp_0'=4,'sp_1'=4,'tp'=16] {'sp_0'}, use_global_device_ids=true, to_apply=%add.1 | all-reduce | flops 16 | bytes 128
  121.3 9.6 %all-gather.8 = f32[4,1,256]{2,1,0:T(1,128)S(1)} all-gather(f32[1,1,256]{2,1,0:T(1,128)S(1)} %bitcast.322), channel_id=9, replica_groups=mesh['sp_0'=4,'sp_1'=4,'tp'=16] {'sp_1'}, dimensions={0}, use_global_device_ids=true | all-gather | bytes 5120 | tf_op jit(solution)/shard_map/all_gather | solution.py:28
  130.9 7.0 %all_gather.84 = f32[4,1,256]{2,1,0:T(1,128)S(1)} all-gather(f32[1,1,256]{2,1,0:T(1,128)S(1)} %get-tuple-element.176), channel_id=1, replica_groups=mesh['sp_0'=4,'sp_1'=4,'tp'=16] {'sp_0'}, dimensions={0}, use_global_device_ids=true | all-gather | bytes 5120 | tf_op jit(solution)/shard_map/all_gather | solution.py:28
  139.3 2.6 multiply_reduce_fusion.1
  141.9 2.2 convolution_convert_fusion.1
  144.7 59.9 %reduce-scatter.3.cloned.1.call-done = bf16[32,2048]{1,0:T(8,128)(2,1)} async-done(((bf16[512,2048]{1,0:T(8,128)(2,1)}), bf16[32,2048]{1,0:T(8,128)(2,1)}) %reduce-scatter.3.cloned.1.call-update) | async-done | bytes 131088 | tf_op jit(solution)/shard_map/reduce_scatter | solution.py:223
  207.4 15.9 %all_to_all.10 = bf16[16,5,2048]{2,1,0:T(8,128)(2,1)S(1)} all-to-all(bf16[16,5,2048]{2,1,0:T(8,128)(2,1)S(1)} %reshape.898), channel_id=1, replica_groups=mesh['sp_0'=4,'sp_1'=4,'tp'=16] {'sp_0','sp_1'}, dimensions={0} | all-to-all | bytes 655360 | tf_op jit(solution)/shard_map/all_to_all | solution.py:250
  224.4 40.1 %all-gather.15.cloned.1.call-done = bf16[1280,2048]{1,0:T(8,128)(2,1)} async-done(((bf16[80,2048]{1,0:T(8,128)(2,1)}), bf16[1280,2048]{1,0:T(8,128)(2,1)}) %all-gather.15.cloned.1.call-update) | async-done | bytes 5242896 | tf_op jit(solution)/shard_map/all_gather | solution.py:253
  264.5 5.1 %fusion.56 = f32[1280,256]{1,0:T(8,128)} fusion(bf16[1280,2048]{1,0:T(8,128)(2,1)} %all-gather.15.cloned.1.call-done, bf16[1,2048,256]{2,1,0:T(8,128)(2,1)S(1)} %copy-done.14), kind=kOutput, calls=%fused_computation.85 | convolution fusion | flops 1342177280 | bytes 7602176 | tf_op jit(solution)/shard_map/dot_general | solution.py:254
  269.6 10.6 %convolution_convert_fusion = bf16[1280,2048]{1,0:T(8,128)(2,1)} fusion(bf16[1280,2048]{1,0:T(8,128)(2,1)} %all-gather.15.cloned.1.call-done, f32[1280,256]{1,0:T(8,128)} %fusion.56, bf16[1,256,2048]{2,1,0:T(8,128)(2,1)S(1)} %copy-done, bf16[1,2048,256]{2,1,0:T(8,128)(2,1)S(1)} %copy-done.15), kind=kOutput, calls=%fused_computation.75 | convolution fusion | flops 2688942080 | bytes 13893632 | tf_op jit(solution)/shard_map/dot_general | solution.py:258
  280.9 63.2 %reduce-scatter.5.cloned.1.call-done = bf16[80,2048]{1,0:T(8,128)(2,1)} async-done(((bf16[1280,2048]{1,0:T(8,128)(2,1)}), bf16[80,2048]{1,0:T(8,128)(2,1)}) %reduce-scatter.5.cloned.1.call-update) | async-done | bytes 327696 | tf_op jit(solution)/shard_map/reduce_scatter | solution.py:257
  344.2 1.9 reshape.900
  346.1 7.3 %all-to-all-start.1 = ((bf16[16,5,2048]{2,1,0:T(8,128)(2,1)}), bf16[16,5,2048]{2,1,0:T(8,128)(2,1)S(1)}, u32[]{:S(2)}, u32[]{:S(2)}) async-start(bf16[16,5,2048]{2,1,0:T(8,128)(2,1)} %reshape.900), calls=%async_computation.3 | async-start | bytes 1048576 | tf_op jit(solution)/shard_map/all_to_all | solution.py:264
  353.4 8.7 %all-to-all-done.1 = bf16[16,5,2048]{2,1,0:T(8,128)(2,1)S(1)} async-done(((bf16[16,5,2048]{2,1,0:T(8,128)(2,1)}), bf16[16,5,2048]{2,1,0:T(8,128)(2,1)S(1)}, u32[]{:S(2)}, u32[]{:S(2)}) %all-to-all-start.1) | async-done | bytes 327712 | tf_op jit(solution)/shard_map/all_to_all | solution.py:264
  363.2 1.8 multiply_reduce_fusion
  (161 shorter events, 32.4 us)
Async XLA Ops:
  6.5 263.0 %copy-start = (bf16[1,256,2048]{2,1,0:T(8,128)(2,1)S(1)}, bf16[1,256,2048]{2,1,0:T(8,128)(2,1)}, u32[]{:S(2)}) copy-start(bf16[1,256,2048]{2,1,0:T(8,128)(2,1)} %param.31) | copy-start | bytes 3145732
  6.5 65.7 %all-gather.17.cloned.1.call-start = ((), (), s32[]{:S(2)}) async-start(), calls=%async_computation.8 | async-start | bytes 1310720 | tf_op jit(solution)/shard_map/all_gather | solution.py:28
  10.0 31.6 %copy-start.17 = (u32[256]{0:T(256)S(1)}, u32[256]{0:T(256)}, u32[]{:S(2)}) copy-start(u32[256]{0:T(256)} %constant.127) | copy-start | bytes 3076
  10.0 64.3 %copy-start.16 = (u32[256]{0:T(256)S(1)}, u32[256]{0:T(256)}, u32[]{:S(2)}) copy-start(u32[256]{0:T(256)} %constant.132) | copy-start | bytes 3076
  10.1 10.8 %copy-start.4 = (bf16[2,1,256,256]{3,2,1,0:T(8,128)(2,1)S(1)}, bf16[2,1,256,256]{3,2,1,0:T(8,128)(2,1)}, u32[]{:S(2)}) copy-start(bf16[2,1,256,256]{3,2,1,0:T(8,128)(2,1)} %get-tuple-element.388) | copy-start | bytes 786436 | tf_op jit(solution)/shard_map/vmap()/while
  10.1 10.8 %copy-start.5 = (bf16[2,1,256,256]{3,2,1,0:T(8,128)(2,1)S(1)}, bf16[2,1,256,256]{3,2,1,0:T(8,128)(2,1)}, u32[]{:S(2)}) copy-start(bf16[2,1,256,256]{3,2,1,0:T(8,128)(2,1)} %get-tuple-element.387) | copy-start | bytes 786436 | tf_op jit(solution)/shard_map/vmap()/while
  10.1 11.3 %copy-start.2 = (bf16[2,1,256,256]{3,2,1,0:T(8,128)(2,1)S(1)}, bf16[2,1,256,256]{3,2,1,0:T(8,128)(2,1)}, u32[]{:S(2)}) copy-start(bf16[2,1,256,256]{3,2,1,0:T(8,128)(2,1)} %get-tuple-element.389) | copy-start | bytes 786436 | tf_op jit(solution)/shard_map/vmap()/while
  22.6 10.8 %copy-start.4 = (bf16[2,1,256,256]{3,2,1,0:T(8,128)(2,1)S(1)}, bf16[2,1,256,256]{3,2,1,0:T(8,128)(2,1)}, u32[]{:S(2)}) copy-start(bf16[2,1,256,256]{3,2,1,0:T(8,128)(2,1)} %get-tuple-element.388) | copy-start | bytes 786436 | tf_op jit(solution)/shard_map/vmap()/while
  22.6 10.8 %copy-start.5 = (bf16[2,1,256,256]{3,2,1,0:T(8,128)(2,1)S(1)}, bf16[2,1,256,256]{3,2,1,0:T(8,128)(2,1)}, u32[]{:S(2)}) copy-start(bf16[2,1,256,256]{3,2,1,0:T(8,128)(2,1)} %get-tuple-element.387) | copy-start | bytes 786436 | tf_op jit(solution)/shard_map/vmap()/while
  22.6 11.3 %copy-start.2 = (bf16[2,1,256,256]{3,2,1,0:T(8,128)(2,1)S(1)}, bf16[2,1,256,256]{3,2,1,0:T(8,128)(2,1)}, u32[]{:S(2)}) copy-start(bf16[2,1,256,256]{3,2,1,0:T(8,128)(2,1)} %get-tuple-element.389) | copy-start | bytes 786436 | tf_op jit(solution)/shard_map/vmap()/while
  35.1 0.7 copy-start.1
  35.1 102.7 %copy-start.9 = (s32[512]{0:T(512)S(1)}, s32[512]{0:T(512)}, u32[]{:S(2)}) copy-start(s32[512]{0:T(512)} %param.23) | copy-start | bytes 6148
  35.2 103.5 %copy-start.3 = (bf16[2,1,256,256]{3,2,1,0:T(8,128)(2,1)S(1)}, bf16[2,1,256,256]{3,2,1,0:T(8,128)(2,1)}, u32[]{:S(2)}) copy-start(bf16[2,1,256,256]{3,2,1,0:T(8,128)(2,1)} %get-tuple-element.404) | copy-start | bytes 786436
  35.9 103.4 %all-gather.13.cloned.1.call-start = ((), (), s32[]{:S(2)}) async-start(), calls=%async_computation.4 | async-start | bytes 1310720 | tf_op jit(solution)/shard_map/all_gather | solution.py:28
  74.3 130.3 %reduce-scatter.3.cloned.1.call-start = ((), (), s32[]{:S(2)}) async-start(), calls=%async_computation.5 | async-start | bytes 2228224 | tf_op jit(solution)/shard_map/reduce_scatter | solution.py:223
  139.3 2.6 copy-start.8
  139.3 2.6 copy-start.13
  141.9 2.3 copy-start.10
  141.9 62.7 %copy-start.6 = (bf16[32,2048]{1,0:T(8,128)(2,1)S(1)}, bf16[32,2048]{1,0:T(8,128)(2,1)}, u32[]{:S(2)}) copy-start(bf16[32,2048]{1,0:T(8,128)(2,1)} %param.17) | copy-start | bytes 393220
  144.1 61.6 %copy-start.11 = (f32[2048]{0:T(1024)S(1)}, f32[2048]{0:T(1024)}, u32[]{:S(2)}) copy-start(f32[2048]{0:T(1024)} %param.26) | copy-start | bytes 24580
  144.1 120.3 %all-gather.15.cloned.1.call-start = ((), (), s32[]{:S(2)}) async-start(), calls=%async_computation.6 | async-start | bytes 5570560 | tf_op jit(solution)/shard_map/all_gather | solution.py:253
  206.9 57.6 %copy-start.14 = (bf16[1,2048,256]{2,1,0:T(8,128)(2,1)S(1)}, bf16[1,2048,256]{2,1,0:T(8,128)(2,1)}, u32[]{:S(2)}) copy-start(bf16[1,2048,256]{2,1,0:T(8,128)(2,1)} %param.29) | copy-start | bytes 3145732
  224.1 45.4 %copy-start.15 = (bf16[1,2048,256]{2,1,0:T(8,128)(2,1)S(1)}, bf16[1,2048,256]{2,1,0:T(8,128)(2,1)}, u32[]{:S(2)}) copy-start(bf16[1,2048,256]{2,1,0:T(8,128)(2,1)} %param.30) | copy-start | bytes 3145732
  224.2 120.0 %reduce-scatter.5.cloned.1.call-start = ((), (), s32[]{:S(2)}) async-start(), calls=%async_computation.7 | async-start | bytes 5570560 | tf_op jit(solution)/shard_map/reduce_scatter | solution.py:257
  280.2 0.7 copy-start.12
  346.1 16.1 %all-to-all-start.1 = ((bf16[16,5,2048]{2,1,0:T(8,128)(2,1)}), bf16[16,5,2048]{2,1,0:T(8,128)(2,1)S(1)}, u32[]{:S(2)}, u32[]{:S(2)}) async-start(bf16[16,5,2048]{2,1,0:T(8,128)(2,1)} %reshape.900), calls=%async_computation.3 | async-start | bytes 1048576 | tf_op jit(solution)/shard_map/all_to_all | solution.py:264
  353.4 11.6 %copy-start.7 = (bf16[32,2048]{1,0:T(8,128)(2,1)S(1)}, bf16[32,2048]{1,0:T(8,128)(2,1)}, u32[]{:S(2)}) copy-start(bf16[32,2048]{1,0:T(8,128)(2,1)} %reduce-scatter.3.cloned.1.call-done) | copy-start | bytes 393220
Sparse Core Ops, SparseCore 0:
  36.0 28.4 all-gather.16
  74.5 28.0 all-gather.12
  144.2 60.3 reduce-scatter.2
  224.3 40.1 all-gather.14
  280.3 63.8 reduce-scatter.4
where the time goes:
time: 374 us; the launch traced here: 372 us
  waiting for transfers between devices  172 us (46%)
  between operations  55.8 us (15%)
  blocking collectives  51.8 us (14%)
  matrix products  30.8 us (8%)
  local copies, waits for them, and re-layouts  25.3 us (7%)
  other arithmetic  23.4 us (6%)
  starting transfers between devices  7.62 us (2%)
  loops' own time  5.4 us (1%)
    reduce_scatter x1, waiting for transfers between devices, on_device(): lax.psum_scatter(jnp.dot(hidden, down_proj[0], preferred_element_type=jnp...  63.2 us
    reduce_scatter x1, waiting for transfers between devices, on_device(): lax.psum_scatter(jnp.dot(head_rows, out_weight, preferred_element_type=jn...  59.9 us
    all_gather x1, waiting for transfers between devices, on_device(): piece = lax.all_gather(arrived, 'tp', axis=0, tiled=True)  40.1 us
    unnamed x2, blocking collectives  19.3 us
    all_gather x2, blocking collectives, carried_in(): pieces = jax.tree.map(lambda part: lax.all_gather(part, axis), running)  16.6 us
    all_to_all x1, blocking collectives, on_device(): lax.all_to_all(outgoing, SP, split_axis=0, concat_axis=0, tiled=True)  15.9 us
    dot_general x1, matrix products, on_device(): jnp.dot(hidden, down_proj[0], preferred_element_type=jnp.float32)  10.6 us
    unnamed x49, local copies, waits for them, and re-layouts  9.59 us
  transfers between devices with their start and end apart: 6, of which 4 were waited for; matrix products, arithmetic and copies ran while one was open for 7% of the time, Pallas kernels for 0%

commit v1 on v0

v1 whole, which is shorter than its diff:
```python
import jax
import jax.numpy as jnp
from jax import lax
from jax.experimental import pallas as pl
from jax.experimental.pallas import tpu as pltpu
from jax.sharding import PartitionSpec as P

MESH = pl.DeviceIdType.MESH
BF16 = jnp.bfloat16
F32 = jnp.float32
MASKED = -1e30
EPSILON = 1e-06
LANES = 128
CAP = 5
SLOTS = 8


def dot(a, b, contract=((1,), (0,))):
    return lax.dot_general(a, b, (contract, ((), ())), preferred_element_type=F32)


def halves_of(x):
    high = x.astype(BF16)
    return high, (x - high.astype(F32)).astype(BF16)


def column(row, extent):
    return jnp.transpose(jnp.broadcast_to(row, (LANES, extent)))


def wide(x, width):
    return jnp.concatenate([x] * (width // LANES), axis=1)


def barrier_with(peers):
    barrier = pltpu.get_barrier_semaphore()
    for peer in peers:
        pl.semaphore_signal(barrier, inc=1, device_id=peer, device_id_type=MESH)
    pl.semaphore_wait(barrier, len(peers))


def exchange_start(n, me, source, target, send_sem, recv_sem):
    copies = []
    for o in range(1, n):
        peer = lax.rem(me + o, n)
        copy = pltpu.make_async_remote_copy(
            src_ref=source.at[peer],
            dst_ref=target.at[me],
            send_sem=send_sem.at[o],
            recv_sem=recv_sem.at[o],
            device_id={"sp": peer},
            device_id_type=MESH,
        )
        copy.start()
        copies.append(copy)
    return copies


def mixer_kernel(
    n_sp,
    q_ref,
    k_ref,
    v_ref,
    in_ref,
    forget_ref,
    doc_ref,
    gain_ref,
    out_ref,
    own_state,
    all_states,
    prefixes,
    arrived,
    num_ref,
    den_ref,
    max_ref,
    send1,
    recv1,
    send2,
    recv2,
):
    me = lax.axis_index("sp")
    extent, head = q_ref.shape
    rows = head // n_sp
    scaling = head ** (-0.5)
    barrier_with([{"sp": lax.rem(me + o, n_sp)} for o in range(1, n_sp)])

    forget = forget_ref[...]
    small = jnp.exp(-jnp.abs(forget))
    above = 1.0 + small
    exact = above - 1.0
    log1p = jnp.where(exact == 0.0, small, jnp.log(above) * (small / jnp.where(exact == 0.0, 1.0, exact)))
    log_forget = jnp.minimum(forget, 0.0) - log1p
    cum = jnp.broadcast_to(log_forget, (8, extent))
    lane = lax.broadcasted_iota(jnp.int32, (8, extent), 1)
    shift = 1
    while shift < extent:
        cum = cum + jnp.where(lane >= shift, pltpu.roll(cum, shift, 1), 0.0)
        shift *= 2
    cum = cum[0:1]
    docs = doc_ref[...].astype(F32)
    base = in_ref[...] - cum
    total = cum[:, extent - 1 : extent]
    first_doc = docs[:, 0:1]
    last_doc = docs[:, extent - 1 : extent]
    log_end = jnp.where(docs == last_doc, total + base, MASKED)
    level = jnp.max(log_end, axis=1, keepdims=True)
    end_weight = column(jnp.exp(log_end - level), extent)
    forget_total = jnp.where(first_doc == last_doc, total, MASKED)

    keys = k_ref[...]
    weighted_values = jnp.concatenate(
        [v_ref[...].astype(F32) * wide(end_weight, head), end_weight], axis=1
    )
    high, low = halves_of(weighted_values)
    state = dot(keys, high, ((0,), (0,))) + dot(keys, low, ((0,), (0,)))
    tail_lane = lax.broadcasted_iota(jnp.int32, (head, LANES), 1)
    tail = state[:, head:]
    for at, scalar in ((1, level), (2, forget_total), (3, first_doc), (4, last_doc)):
        tail = jnp.where(tail_lane == at, scalar, tail)
    own_state[:, :, :head] = state[:, :head].reshape(n_sp, rows, head)
    own_state[:, :, head:] = tail.reshape(n_sp, rows, LANES)
    sends = exchange_start(n_sp, me, own_state, all_states, send1, recv1)
    all_states[me] = own_state[me]

    cum_col = column(cum, extent)
    doc_col = column(docs, extent)
    block = LANES
    for i in range(extent // block):
        here = slice(i * block, (i + 1) * block)
        width = (i + 1) * block
        scores = dot(q_ref[here, :], k_ref[:width, :], ((1,), (1,))) * scaling
        permitted = wide(doc_col[here], width) == docs[:, :width]
        row_at = lax.broadcasted_iota(jnp.int32, (block, width), 0) + i * block
        col_at = lax.broadcasted_iota(jnp.int32, (block, width), 1)
        permitted = permitted & (row_at >= col_at)
        logs = jnp.where(permitted, wide(cum_col[here], width) + base[:, :width], MASKED)
        row_max = jnp.max(logs, axis=1, keepdims=True)
        weighted = scores * jnp.exp(logs - row_max)
        num_ref[here, :] = dot(weighted.astype(BF16), v_ref[:width, :])
        den_ref[here, :] = jnp.broadcast_to(jnp.sum(weighted, axis=1, keepdims=True), (block, LANES))
        max_ref[here, :] = jnp.broadcast_to(row_max, (block, LANES))

    for copy in sends:
        copy.wait()
    running = jnp.zeros((rows, head + LANES), F32)
    running_level = jnp.full((rows, 1), MASKED, F32)
    running_doc = jnp.full((rows, 1), -1.0, F32)
    slice_lane = lax.broadcasted_iota(jnp.int32, (rows, LANES), 1)
    for j in range(n_sp):
        piece = all_states[j]
        piece_level = piece[:, head + 1 : head + 2]
        piece_forget = piece[:, head + 2 : head + 3]
        piece_first = piece[:, head + 3 : head + 4]
        in_level = jnp.where(running_doc == piece_first, running_level, MASKED)
        prefixes[j, :, :head] = running[:, :head]
        prefixes[j, :, head:] = jnp.where(slice_lane == 1, in_level, running[:, head:])
        passed = in_level + piece_forget
        running_level = jnp.maximum(passed, piece_level)
        running = jnp.exp(passed - running_level) * running + jnp.exp(piece_level - running_level) * jnp.concatenate(
            [piece[:, :head], jnp.where(slice_lane == 0, piece[:, head:], 0.0)], axis=1
        )
        running_doc = piece[:, head + 4 : head + 5]
    sends = exchange_start(n_sp, me, prefixes, arrived, send2, recv2)
    arrived[me] = prefixes[me]
    for copy in sends:
        copy.wait()

    in_level = arrived[0][0:1, head + 1 : head + 2]
    high, low = halves_of(arrived[...].reshape(head, head + LANES))
    gain = gain_ref[...]
    for i in range(extent // block):
        here = slice(i * block, (i + 1) * block)
        far = (dot(q_ref[here, :], high) + dot(q_ref[here, :], low)) * scaling
        carried = jnp.where(doc_col[here] == first_doc, cum_col[here] + in_level, MASKED)
        row_max = max_ref[here, :]
        new_max = jnp.maximum(row_max, carried)
        own_share = jnp.exp(row_max - new_max)
        far_share = jnp.exp(carried - new_max)
        numerator = wide(own_share, head) * num_ref[here, :] + wide(far_share, head) * far[:, :head]
        denominator = own_share * den_ref[here, :] + far_share * far[:, head : head + 1]
        bound = jnp.maximum(jnp.abs(denominator), jnp.exp(-new_max))
        mixed = numerator / wide(bound, head)
        scale = lax.rsqrt(jnp.mean(mixed * mixed, axis=1, keepdims=True) + EPSILON)
        out_ref[here, :] = (mixed * scale * gain).astype(BF16)


def ring_chains(n_z):
    far, near = n_z // 2, n_z // 2 - 1
    return ((1, 0, far), (1, 1, near), (-1, 0, near), (-1, 1, far))


def reduce_ring(n_z, z, core, part, half, out, inc, send_sem, recv_sem):
    chains = ring_chains(n_z)
    sent = {}
    for i in range(1, n_z // 2 + 1):
        for c, (way, h, steps) in enumerate(chains):
            if i > steps:
                continue
            cols = slice(h * half, (h + 1) * half)
            dest = lax.rem(z + way * (steps - i + 1) + n_z, n_z)
            value = part[dest, :, cols]
            if i > 1:
                sent[c, i - 1].wait_recv()
                value = value + inc[c, i - 2].astype(F32)
            out[c, i - 1] = value.astype(BF16)
            copy = pltpu.make_async_remote_copy(
                src_ref=out.at[c, i - 1],
                dst_ref=inc.at[c, i - 1],
                send_sem=send_sem.at[c, i - 1],
                recv_sem=recv_sem.at[c, i - 1],
                device_id={"tp": 2 * lax.rem(z + way + n_z, n_z) + core},
                device_id_type=MESH,
            )
            copy.start()
            sent[c, i] = copy
    sums = []
    for h in range(2):
        value = part[z, :, h * half : (h + 1) * half]
        for c, (way, chain_half, steps) in enumerate(chains):
            if chain_half == h:
                sent[c, steps].wait_recv()
                value = value + inc[c, steps - 1].astype(F32)
        sums.append(value)
    for copy in sent.values():
        copy.wait_send()
    return jnp.concatenate(sums, axis=1)


def expert_kernel(
    n_sp,
    n_z,
    heads_ref,
    residual_ref,
    norm_gain_ref,
    ids_ref,
    weights_ref,
    out_weight_ref,
    gate_ref,
    up_ref,
    down_ref,
    result_ref,
    w_out,
    w_gate,
    w_up,
    w_down,
    heads_in,
    part1,
    rs1_out,
    rs1_in,
    outgoing,
    incoming,
    gathered,
    part2,
    rs2_out,
    rs2_in,
    leaving,
    returned,
    local_sem,
    pair_send,
    pair_recv,
    rs1_send,
    rs1_recv,
    a2a_send,
    a2a_recv,
    ag_send,
    ag_recv,
    rs2_send,
    rs2_recv,
    back_send,
    back_recv,
):
    sp = lax.axis_index("sp")
    tp = lax.axis_index("tp")
    z = tp // 2
    core = tp - 2 * z
    sibling = {"tp": 2 * z + 1 - core}
    width = residual_ref.shape[1]
    half = width // 2
    tokens = residual_ref.shape[0]
    peers = [{"sp": lax.rem(sp + o, n_sp)} for o in range(1, n_sp)]
    peers += [sibling]
    peers += [{"tp": 2 * lax.rem(z + way + n_z, n_z) + core} for way in (1, -1)]
    barrier_with(peers)

    pair = []
    own = []
    moved = (
        (heads_ref.at[:, 1 - core], heads_in),
        (out_weight_ref, w_out.at[1]),
        (gate_ref, w_gate.at[1]),
        (up_ref, w_up.at[1]),
        (down_ref, w_down.at[1]),
    )
    for at, (source, target) in enumerate(moved):
        copy = pltpu.make_async_remote_copy(
            src_ref=source,
            dst_ref=target,
            send_sem=pair_send.at[at],
            recv_sem=pair_recv.at[at],
            device_id=sibling,
            device_id_type=MESH,
        )
        copy.start()
        pair.append(copy)
    for at, (source, target) in enumerate(
        (
            (out_weight_ref, w_out.at[0]),
            (gate_ref, w_gate.at[0]),
            (up_ref, w_up.at[0]),
            (down_ref, w_down.at[0]),
        )
    ):
        copy = pltpu.make_async_copy(source, target, local_sem.at[at])
        copy.start()
        own.append(copy)

    lane = lax.broadcasted_iota(jnp.int32, (tokens, LANES), 1)
    chosen = [ids_ref[:, k : k + 1] == lane for k in range(2)]
    either = jnp.where(chosen[0] | chosen[1], 1.0, 0.0)
    before = jnp.where(
        lax.broadcasted_iota(jnp.int32, (tokens, tokens), 0)
        > lax.broadcasted_iota(jnp.int32, (tokens, tokens), 1),
        1.0,
        0.0,
    )
    earlier = dot(before.astype(BF16), either.astype(BF16))
    select = []
    for k in range(2):
        rank = jnp.sum(jnp.where(chosen[k], earlier, 0.0), axis=1, keepdims=True)
        slot = ids_ref[:, k : k + 1].astype(F32) * SLOTS + rank
        select.append(jnp.where(slot == lane.astype(F32), 1.0, 0.0))

    own[0].wait()
    pair[0].wait()
    pair[1].wait()
    mine = heads_ref[:, core].reshape(n_z * tokens, -1)
    theirs = heads_in[...].reshape(n_z * tokens, -1)
    chunk = 512
    for at in range(0, width, chunk):
        cols = slice(at, at + chunk)
        part1[:, :, cols] = (dot(mine, w_out[0, :, cols]) + dot(theirs, w_out[1, :, cols])).reshape(
            n_z, tokens, chunk
        )
    update = reduce_ring(n_z, z, core, part1, half, rs1_out, rs1_in, rs1_send, rs1_recv)
    stream = residual_ref[...].astype(F32) + update
    normed = stream * lax.rsqrt(jnp.mean(stream * stream, axis=1, keepdims=True) + EPSILON)
    normed = (normed * norm_gain_ref[...]).astype(BF16)

    placed = dot((select[0] + select[1]).astype(BF16), normed, ((0,), (0,)))
    outgoing[...] = placed.reshape(n_sp, SLOTS, width).astype(BF16)
    sends = exchange_start(n_sp, sp, outgoing, incoming, a2a_send, a2a_recv)
    incoming[sp] = outgoing[sp]
    for copy in own[1:] + pair[2:]:
        copy.wait()
    for copy in sends:
        copy.wait()

    packed = n_sp * CAP
    padded = n_sp * SLOTS
    row = lax.broadcasted_iota(jnp.int32, (packed, padded), 0)
    col = lax.broadcasted_iota(jnp.int32, (packed, padded), 1)
    inside = jnp.bitwise_and(col, SLOTS - 1)
    source_row = jnp.right_shift(col, 3) * CAP + inside
    pack = jnp.where((source_row == row) & (inside < CAP), 1.0, 0.0).astype(BF16)
    padded_rows = incoming[...].astype(F32).reshape(padded, width).astype(BF16)
    packed_rows = dot(pack, padded_rows).astype(BF16)
    gathered[z, 0] = packed_rows[:, :half]
    gathered[z, 1] = packed_rows[:, half:]

    chains = ring_chains(n_z)
    gathers = {}

    def forward(c, i):
        way, h, steps = chains[c]
        if i > steps:
            return
        origin = lax.rem(z - way * (i - 1) + n_z, n_z)
        copy = pltpu.make_async_remote_copy(
            src_ref=gathered.at[origin, h],
            dst_ref=gathered.at[origin, h],
            send_sem=ag_send.at[c, i - 1],
            recv_sem=ag_recv.at[c, i - 1],
            device_id={"tp": 2 * lax.rem(z + way + n_z, n_z) + core},
            device_id_type=MESH,
        )
        copy.start()
        gathers[c, i] = copy

    def experts(origin):
        left = gathered[origin, 0]
        right = gathered[origin, 1]
        total = None
        for s in range(2):
            gate = dot(left, w_gate[s, :half, :]) + dot(right, w_gate[s, half:, :])
            up = dot(left, w_up[s, :half, :]) + dot(right, w_up[s, half:, :])
            hidden = (gate / (1.0 + jnp.exp(-gate)) * up).astype(BF16)
            down = dot(hidden, w_down[s])
            total = down if total is None else total + down
        part2[origin] = total

    for c in range(4):
        forward(c, 1)
    experts(z)
    for i in range(1, n_z // 2 + 1):
        for c, (way, h, steps) in enumerate(chains):
            if i <= steps:
                gathers[c, i].wait_recv()
                forward(c, i + 1)
        experts(lax.rem(z - i + n_z, n_z))
        if i < n_z // 2:
            experts(lax.rem(z + i, n_z))
    summed = reduce_ring(n_z, z, core, part2, half, rs2_out, rs2_in, rs2_send, rs2_recv)
    for copy in gathers.values():
        copy.wait_send()

    row = lax.broadcasted_iota(jnp.int32, (padded, packed), 0)
    col = lax.broadcasted_iota(jnp.int32, (padded, packed), 1)
    inside = jnp.bitwise_and(row, SLOTS - 1)
    source_row = jnp.right_shift(row, 3) * CAP + inside
    unpack = jnp.where((source_row == col) & (inside < CAP), 1.0, 0.0).astype(BF16)
    spread = dot(unpack, summed.astype(BF16))
    leaving[...] = spread.reshape(n_sp, SLOTS, width).astype(BF16)
    sends = exchange_start(n_sp, sp, leaving, returned, back_send, back_recv)
    returned[sp] = leaving[sp]
    for copy in sends:
        copy.wait()
    back = returned[...].astype(F32).reshape(padded, width).astype(BF16)
    total = stream
    for k in range(2):
        total = total + weights_ref[:, k : k + 1] * dot(select[k].astype(BF16), back)
    result_ref[...] = total.astype(BF16)


def on_device(
    n_sp,
    n_tp,
    residual,
    queries,
    keys,
    values,
    in_gate,
    forget_gate,
    doc_ids,
    head_gain,
    out_weight,
    norm_gain,
    route_ids,
    route_weights,
    gate_proj,
    up_proj,
    down_proj,
):
    extent, head = queries.shape
    rows = head // n_sp
    n_z = n_tp // 2
    tokens, width = residual.shape
    units = gate_proj.shape[2]
    vmem = pl.BlockSpec(memory_space=pltpu.VMEM)
    anywhere = pl.BlockSpec(memory_space=pl.ANY)
    dma = pltpu.SemaphoreType.DMA

    def body(*refs):
        mixer_kernel(n_sp, *refs)

    head_rows = pl.pallas_call(
        body,
        name="mixer",
        out_shape=jax.ShapeDtypeStruct((extent, head), BF16),
        in_specs=[vmem] * 7,
        out_specs=vmem,
        scratch_shapes=[pltpu.VMEM((n_sp, rows, head + LANES), F32)] * 4
        + [
            pltpu.VMEM((extent, head), F32),
            pltpu.VMEM((extent, LANES), F32),
            pltpu.VMEM((extent, LANES), F32),
        ]
        + [dma((n_sp,))] * 4,
        compiler_params=pltpu.CompilerParams(
            collective_id=0, has_side_effects=True, vmem_limit_bytes=48 << 20
        ),
    )(
        queries,
        keys,
        values,
        in_gate,
        forget_gate,
        doc_ids.reshape(1, extent),
        head_gain.reshape(1, head),
    )

    def body2(*refs):
        expert_kernel(n_sp, n_z, *refs)

    half = width // 2
    packed = n_sp * CAP
    steps = n_z // 2
    return pl.pallas_call(
        body2,
        name="experts",
        out_shape=jax.ShapeDtypeStruct((tokens, width), BF16),
        in_specs=[vmem] * 5 + [anywhere] * 4,
        out_specs=vmem,
        scratch_shapes=[
            pltpu.VMEM((2, head, width), BF16),
            pltpu.VMEM((2, width, units), BF16),
            pltpu.VMEM((2, width, units), BF16),
            pltpu.VMEM((2, units, width), BF16),
            pltpu.VMEM((n_z, tokens, head), BF16),
            pltpu.VMEM((n_z, tokens, width), F32),
            pltpu.VMEM((4, steps, tokens, half), BF16),
            pltpu.VMEM((4, steps, tokens, half), BF16),
            pltpu.VMEM((n_sp, SLOTS, width), BF16),
            pltpu.VMEM((n_sp, SLOTS, width), BF16),
            pltpu.VMEM((n_z, 2, packed, half), BF16),
            pltpu.VMEM((n_z, packed, width), F32),
            pltpu.VMEM((4, steps, packed, half), BF16),
            pltpu.VMEM((4, steps, packed, half), BF16),
            pltpu.VMEM((n_sp, SLOTS, width), BF16),
            pltpu.VMEM((n_sp, SLOTS, width), BF16),
            dma((4,)),
            dma((5,)),
            dma((5,)),
            dma((4, steps)),
            dma((4, steps)),
            dma((n_sp,)),
            dma((n_sp,)),
            dma((4, steps)),
            dma((4, steps)),
            dma((4, steps)),
            dma((4, steps)),
            dma((n_sp,)),
            dma((n_sp,)),
        ],
        compiler_params=pltpu.CompilerParams(
            collective_id=1, has_side_effects=True, vmem_limit_bytes=60 << 20
        ),
    )(
        head_rows.reshape(n_z, 2, tokens, head),
        residual,
        norm_gain.reshape(1, width),
        route_ids,
        route_weights,
        out_weight,
        gate_proj[0],
        up_proj[0],
        down_proj[0],
    )


def solution(mesh):
    n_sp, n_tp = mesh.shape["sp"], mesh.shape["tp"]
    both = ("sp", "tp")

    def step(*args):
        return on_device(n_sp, n_tp, *args)

    return jax.shard_map(
        step,
        mesh=mesh,
        in_specs=(
            P(both, None),
            P("sp", "tp"),
            P("sp", "tp"),
            P("sp", "tp"),
            P("tp", "sp"),
            P("tp", "sp"),
            P("sp"),
            P("tp"),
            P("tp", None),
            P(),
            P(both, None),
            P(both, None),
            P("sp", None, "tp"),
            P("sp", None, "tp"),
            P("sp", "tp", None),
        ),
        out_specs=P(both, None),
        check_vma=False,
    )
```

time: 374 us -> 133 us (0.36)
  waiting for transfers between devices: 172 us -> 0 us
  Pallas kernels: 0 us -> 124 us
  between operations: 55.8 us -> 0.05 us
  blocking collectives: 51.8 us -> 0 us
  matrix products: 30.8 us -> 0 us
  other arithmetic: 23.4 us -> 0 us
  local copies, waits for them, and re-layouts: 25.3 us -> 7.19 us
  starting transfers between devices: 7.62 us -> 0 us
  loops' own time: 5.4 us -> 0 us
    pallas_call x0 -> x2, Pallas kernels: none -> 124 us  [the longest x1 104 us: on_device(): pl.pallas_call(body2, name='experts', out_shape=jax.ShapeDtypeStruct((tok...]
    reduce_scatter x2 -> x0, waiting for transfers between devices: 123 us -> none  [the longest x1 63.2 us: on_device(): lax.psum_scatter(jnp.dot(hidden, down_proj[0], preferred_element_type=jnp...]
    all_gather x3 -> x0, waiting for transfers between devices: 40.1 us -> none  [the longest x1 40.1 us: on_device(): piece = lax.all_gather(arrived, 'tp', axis=0, tiled=True)]
    dot_general x18 -> x0, matrix products: 30.8 us -> none  [the longest x1 10.6 us: on_device(): jnp.dot(hidden, down_proj[0], preferred_element_type=jnp.float32)]
    unnamed x2 -> x0, blocking collectives: 19.3 us -> none
    all_gather x2 -> x0, blocking collectives: 16.6 us -> none  [carried_in(): pieces = jax.tree.map(lambda part: lax.all_gather(part, axis), running)]
    all_to_all x1 -> x0, blocking collectives: 15.9 us -> none  [on_device(): lax.all_to_all(outgoing, SP, split_axis=0, concat_axis=0, tiled=True)]
    all_to_all x1 -> x0, waiting for transfers between devices: 8.75 us -> none  [on_device(): lax.all_to_all(expert_out, SP, split_axis=0, concat_axis=0, tiled=True)]
  transfers between devices with their start and end apart: 6 -> 0, of which waited for: 4 -> 0; matrix products, arithmetic and copies ran while one was open for 7% -> 0% of each run, Pallas kernels for 0% -> 0%
where the time goes in v1:
time: 133 us; the launch traced here: 132 us
  Pallas kernels  124 us (93%)
  local copies, waits for them, and re-layouts  7.19 us (5%)
    pallas_call x1, Pallas kernels, on_device(): pl.pallas_call(body2, name='experts', out_shape=jax.ShapeDtypeStruct((tok...  104 us
    pallas_call x1, Pallas kernels, on_device(): pl.pallas_call(body, name='mixer', out_shape=jax.ShapeDtypeStruct((extent...  20.7 us
    unnamed x23, local copies, waits for them, and re-layouts  7.19 us

profile of v1, /device:TPU:2, one launch (start us, length us, event | category | flops | bytes accessed | tf_op | source)
XLA Modules:
  0.0 131.6 jit_solution(17389445313813642275)
XLA Ops:
  0.0 0.0 copy-start.8
  0.0 0.7 copy-done.8
  0.7 0.0 copy-start.9
  0.7 0.7 copy.16.refs_3_
  1.4 0.0 copy-done.9
  1.4 0.0 copy-start.4
  1.4 0.0 copy-start.5
  1.4 0.0 copy-start.6
  1.4 0.0 copy-start.7
  1.4 0.7 copy.17.refs_4_
  2.1 0.0 copy-done.4
  2.1 0.0 copy-done.5
  2.1 0.0 copy-done.6
  2.1 0.0 copy-done.7
  2.1 0.0 copy-start.1
  2.1 0.9 copy-done.1
  3.1 0.0 copy-start.2
  3.1 0.9 copy-done.2
  4.0 0.0 copy-start.3
  4.0 0.9 copy-done.3
  5.0 20.7 %mixer.1 = bf16[512,256]{1,0:T(8,128)(2,1)S(1)} custom-call(bf16[512,256]{1,0:T(8,128)(2,1)S(1)} %copy-done.1, bf16[512,256]{1,0:T(8,128)(2,1)S(1)} %copy-done.2, bf16[512,256]{1,0:T(8,128)(2,1)S(1)} %copy-done.3, f32[1,512]{1,0:T(1,128)S(1)} %copy-done.4, f32[1,512]{1,0:T(1,128)S(1)} %copy-done.5, s32[1,512]{1,0:T(1,128)S(1)} %bitcast.8, f32[1,256]{1,0:T(1,128)S(1)} %bitcast.9), custom_call_target="tpu_custom_call" | custom-call | tf_op jit(solution)/shard_map/mixer/pallas_call | solution.py:465
  25.7 0.0 copy-start
  25.7 0.7 copy-done
  26.4 103.7 %experts.1 = bf16[32,2048]{1,0:T(8,128)(2,1)} custom-call(bf16[8,2,32,256]{3,2,1,0:T(8,128)(2,1)} %bitcast.7, bf16[32,2048]{1,0:T(8,128)(2,1)} %refs_1_.3, f32[1,2048]{1,0:T(1,128)} %bitcast.13, s32[32,2]{1,0:T(8,128)} %copy.16.refs_3_, f32[32,2]{1,0:T(8,128)} %copy.17.refs_4_, bf16[256,2048]{1,0:T(8,128)(2,1)} %refs_5_.1, bf16[2048,256]{1,0:T(8,128)(2,1)} %bitcast.10, ...), custom_call_target="tpu_custom_call" | custom-call | tf_op jit(solution)/shard_map/experts/pallas_call | solution.py:497
  130.0 1.6 %copy.19 = bf16[32,2048]{1,0:T(8,128)(2,1)} copy(bf16[32,2048]{1,0:T(8,128)(2,1)} %experts.1) | data formatting | bytes 262144
Async XLA Ops:
  0.0 0.7 copy-start.8
  0.7 0.7 copy-start.9
  1.4 0.7 copy-start.4
  1.4 0.7 copy-start.5
  1.4 0.7 copy-start.6
  1.4 0.7 copy-start.7
  2.1 1.0 copy-start.1
  3.1 0.9 copy-start.2
  4.0 0.9 copy-start.3
  25.7 0.7 copy-start
